TPU v7x, 32 devices: a whole 2x2x4 slice. The times are simulated.
32 devices in a mesh: rep: 2 (over x), fs: 8 (over z, y), tp: 2 (over core).
Axes of the slice: x: 2, y: 2, z: 4, core: 2. Of those that a mesh axis runs over, the one named last changes fastest.
Arguments:
- activations: bfloat16 [16384, 1024], P(('rep', 'fs', 'tp')), may hold values from -8 to 8
- mixer_gain: float32 [1024], replicated, may hold values from 0.1 to 1.9
- query_weight: bfloat16 [1024, 256], P('fs', 'tp'), may hold values from -0.1875 to 0.1875
- key_weight: bfloat16 [1024, 256], P('fs', 'tp'), may hold values from -0.1875 to 0.1875
- value_weight: bfloat16 [1024, 512], P('fs', 'tp'), may hold values from -0.1875 to 0.1875
- rank_weight: bfloat16 [1024, 16], replicated, may hold values from -0.1875 to 0.1875
- decay_gate_weight: bfloat16 [16, 256], P(None, 'tp'), may hold values from -1.5 to 1.5
- decay_gate_bias: float32 [256], P('tp'), may hold values from -1.5 to 8
- head_gain: float32 [256], replicated, may hold values from 0.1 to 1.9
- output_weight: bfloat16 [512, 1024], P('tp', 'fs'), may hold values from -0.25 to 0.25
- ffn_gain: float32 [1024], replicated, may hold values from 0.1 to 1.9
- gate_weight: bfloat16 [1024, 2816], P('fs', 'tp'), may hold values from -0.1875 to 0.1875
- up_weight: bfloat16 [1024, 2816], P('fs', 'tp'), may hold values from -0.1875 to 0.1875
- down_weight: bfloat16 [2816, 1024], P('tp', 'fs'), may hold values from -0.109375 to 0.109375
Outputs:
- result: bfloat16 [16384, 1024], P(('rep', 'fs', 'tp'))
All inputs are finite; a program needn't handle non-finite values.
Results may differ from a plain program's by a relative error of at most 0.0056.
Values may be sent and summed in bfloat16 or wider, within the bound.
No kernel may reach another device: no remote copies, remote signals or barrier semaphores. Data moves between devices by JAX's collectives and lax.ppermute only.
A program may use at most 64 MiB of HBM per device.

v0:
```python
import jax
import jax.numpy as jnp
from jax import lax
from jax.sharding import PartitionSpec as P

DK = 128
DV = 256
BLOCK = 64
epsilon = 1e-06
decay_softness = 16.0
highest = lax.Precision.HIGHEST


def rms_scale(values, gains):
    return values * lax.rsqrt(jnp.mean(values * values, axis=-1, keepdims=True) + epsilon) * gains


def linear_attention(queries, keys_all, values_all, decay_logarithm, head_count):
    length = queries.shape[0]
    number = length // BLOCK
    halfway = BLOCK // 2
    causal = jnp.tril(jnp.ones((BLOCK, BLOCK), bool))

    def to_blocks(matrix):
        return matrix.astype(jnp.float32).reshape(
            number, BLOCK, head_count, matrix.shape[1] // head_count
        )

    block_query = to_blocks(queries)
    block_key = to_blocks(keys_all)
    block_value = to_blocks(values_all)
    cumulative = jnp.cumsum(to_blocks(decay_logarithm), axis=1)
    middle = cumulative[:, halfway - 1 : halfway]
    query_local = block_query * jnp.exp(cumulative - middle)
    key_local = block_key * jnp.exp(middle - cumulative)
    scores = jnp.einsum("nthd,nshd->nhts", query_local, key_local, precision=highest)
    scores = jnp.where(causal[None, None], scores, 0.0)
    within = jnp.einsum("nhts,nshv->nthv", scores, block_value, precision=highest)
    lasting = cumulative[:, -1]
    update = jnp.einsum(
        "nshd,nshv->nhdv",
        block_key * jnp.exp(lasting[:, None] - cumulative),
        block_value,
        precision=highest,
    )

    def advance(memory, inputs):
        fade, addition = inputs
        return (jnp.exp(fade)[:, :, None] * memory + addition, memory)

    key_width = queries.shape[1] // head_count
    value_width = values_all.shape[1] // head_count
    initial = jnp.zeros((head_count, key_width, value_width), jnp.float32)
    earlier = lax.scan(advance, initial, (lasting, update))[1]
    carried = jnp.einsum(
        "nthd,nhdv->nthv", block_query * jnp.exp(cumulative), earlier, precision=highest
    )
    return (within + carried).reshape(length, head_count, value_width)


def project_inputs(source, weight):
    return jnp.dot(source, weight, preferred_element_type=jnp.float32)


def local(
    activations,
    mixer_gain,
    query_weight,
    key_weight,
    value_weight,
    rank_weight,
    decay_gate_weight,
    decay_gate_bias,
    head_gain,
    output_weight,
    ffn_gain,
    gate_weight,
    up_weight,
    down_weight,
):
    residual = activations.astype(jnp.float32)
    normed = rms_scale(residual, mixer_gain).astype(jnp.bfloat16)
    rank_slice = project_inputs(normed, rank_weight).astype(jnp.bfloat16)
    sequence, rank_slices_gathered = (
        lax.all_gather(normed, "tp", axis=0, tiled=True),
        lax.all_gather(rank_slice, "tp", axis=0, tiled=True),
    )
    length = sequence.shape[0]
    query_full, key_full, value_full = (
        lax.all_gather(query_weight, "fs", axis=0, tiled=True),
        lax.all_gather(key_weight, "fs", axis=0, tiled=True),
        lax.all_gather(value_weight, "fs", axis=0, tiled=True),
    )
    queries = project_inputs(sequence, query_full).astype(jnp.bfloat16)
    keys_all = project_inputs(sequence, key_full).astype(jnp.bfloat16)
    values_all = project_inputs(sequence, value_full).astype(jnp.bfloat16)
    decay_logarithm = (
        jax.nn.log_sigmoid(
            project_inputs(rank_slices_gathered, decay_gate_weight) + decay_gate_bias
        )
        / decay_softness
    )
    head_count = query_weight.shape[1] // DK
    attended = linear_attention(queries, keys_all, values_all, decay_logarithm, head_count)
    head_rows = rms_scale(attended, head_gain).astype(jnp.bfloat16).reshape(length, head_count * DV)
    own_rows = lax.all_to_all(head_rows, "tp", split_axis=0, concat_axis=1, tiled=True)
    tall_out = lax.all_gather(output_weight, "tp", axis=0, tiled=True)
    whole_out = lax.all_gather(tall_out, "fs", axis=1, tiled=True)
    mixed = residual + project_inputs(own_rows, whole_out)
    ffn_normed = rms_scale(mixed, ffn_gain).astype(jnp.bfloat16)
    ffn_sequence = lax.all_gather(ffn_normed, "tp", axis=0, tiled=True)
    gate_full, up_full = (
        lax.all_gather(gate_weight, "fs", axis=0, tiled=True),
        lax.all_gather(up_weight, "fs", axis=0, tiled=True),
    )
    down_full = lax.all_gather(down_weight, "fs", axis=1, tiled=True)
    hidden = (
        jax.nn.silu(project_inputs(ffn_sequence, gate_full)) * project_inputs(ffn_sequence, up_full)
    ).astype(jnp.bfloat16)
    result = mixed + lax.psum_scatter(
        project_inputs(hidden, down_full).astype(jnp.bfloat16),
        "tp",
        scatter_dimension=0,
        tiled=True,
    ).astype(jnp.float32)
    return result.astype(jnp.bfloat16)


def solution(mesh):
    in_specs = (
        P(("rep", "fs", "tp"), None),
        P(),
        P("fs", "tp"),
        P("fs", "tp"),
        P("fs", "tp"),
        P(),
        P(None, "tp"),
        P("tp"),
        P(),
        P("tp", "fs"),
        P(),
        P("fs", "tp"),
        P("fs", "tp"),
        P("tp", "fs"),
    )
    out_specs = P(("rep", "fs", "tp"), None)
    return jax.shard_map(local, mesh=mesh, in_specs=in_specs, out_specs=out_specs, check_vma=False)
```

profile of v0, /device:TPU:0, one launch (start us, length us, event | category | flops | bytes accessed | tf_op | source)
XLA Modules:
  0.0 369.9 jit_solution(17549334003282702146)
XLA Ops:
  6.5 1.5 fusion.2
  8.1 2.5 fusion.4
  10.7 2.2 all_gather.38
  13.0 1.6 convolution_convert_fusion.3
  14.6 2.1 all_gather.36
  17.6 32.6 %all_gather.37 = bf16[1024,128]{1,0:T(8,128)(2,1)S(1)} all-gather(bf16[128,128]{1,0:T(8,128)(2,1)S(1)} %copy-done.8), channel_id=1, replica_groups=mesh['rep'=2,'fs'=8,'tp'=2] {'fs'}, dimensions={0}, use_global_device_ids=true | all-gather | bytes 294912 | tf_op jit(solution)/shard_map/all_gather | solution.py:91
  50.2 31.1 %all_gather.35 = bf16[1024,128]{1,0:T(8,128)(2,1)S(1)} all-gather(bf16[128,128]{1,0:T(8,128)(2,1)S(1)} %copy-done.9), channel_id=1, replica_groups=mesh['rep'=2,'fs'=8,'tp'=2] {'fs'}, dimensions={0}, use_global_device_ids=true | all-gather | bytes 294912 | tf_op jit(solution)/shard_map/all_gather | solution.py:90
  81.3 31.3 %all_gather.34 = bf16[1024,256]{1,0:T(8,128)(2,1)S(1)} all-gather(bf16[128,256]{1,0:T(8,128)(2,1)S(1)} %copy-done.7), channel_id=1, replica_groups=mesh['rep'=2,'fs'=8,'tp'=2] {'fs'}, dimensions={0}, use_global_device_ids=true | all-gather | bytes 589824 | tf_op jit(solution)/shard_map/all_gather | solution.py:92
  112.6 2.4 convolution_convert_fusion.1
  115.8 1.6 fusion.14
  119.2 12.6 %while.13 = (s32[]{:T(128)}, f32[1,128,256]{2,1,0:T(8,128)S(1)}, f32[16,1,128,256]{3,2,1,0:T(8,128)}, f32[16,1,128]{2,1,0:T(1,128)S(1)}, f32[16,1,128,256]{3,2,1,0:T(8,128)S(1)}, /*index=5*/s32[]{:T(128)}, s32[]{:T(128)}) while((s32[]{:T(128)}, f32[1,128,256]{2,1,0:T(8,128)S(1)}, f32[16,1,128,256]{3,2,1,0:T(8,128)}, ...), condition=%wide.region_3.4_spmd.clone, body=%wide.region_2.3_spmd.clone.sunk | while | flops 131075 | bytes 657504 | solution.py:54
  131.8 2.2 convolution_select_fusion
  134.1 3.0 fusion.5
  139.2 3.5 all-to-all-start
  142.8 1.7 all-to-all-done
  145.2 2.2 multiply_reduce_fusion
  150.7 10.0 %all-gather.11.cloned.1.call-done = bf16[1024,1024]{1,0:T(8,128)(2,1)} async-done(((bf16[512,1024]{1,0:T(8,128)(2,1)}), bf16[1024,1024]{1,0:T(8,128)(2,1)}) %all-gather.11.cloned.1.call-update) | async-done | bytes 2097168 | tf_op jit(solution)/shard_map/all_gather | solution.py:111
  160.7 60.5 %all-gather.13.cloned.1.call-done = bf16[1024,1408]{1,0:T(8,128)(2,1)} async-done(((bf16[128,1408]{1,0:T(8,128)(2,1)}), bf16[1024,1408]{1,0:T(8,128)(2,1)}) %all-gather.13.cloned.1.call-update) | async-done | bytes 2883600 | tf_op jit(solution)/shard_map/all_gather | solution.py:113
  221.2 8.3 %fusion.27 = f32[1024,1408]{1,0:T(8,128)} fusion(bf16[1024,1024]{1,0:T(8,128)(2,1)} %all-gather.11.cloned.1.call-done, bf16[1024,1408]{1,0:T(8,128)(2,1)} %all-gather.13.cloned.1.call-done), kind=kOutput, calls=%fused_computation.58 | convolution fusion | flops 2952790016 | bytes 10747904 | tf_op jit(solution)/shard_map/dot_general | solution.py:62
  229.6 49.6 %all-gather.15.cloned.1.call-done = bf16[1024,1408]{1,0:T(8,128)(2,1)} async-done(((bf16[128,1408]{1,0:T(8,128)(2,1)}), bf16[1024,1408]{1,0:T(8,128)(2,1)}) %all-gather.15.cloned.1.call-update) | async-done | bytes 2883600 | tf_op jit(solution)/shard_map/all_gather | solution.py:114
  279.2 60.1 %all-gather.17.cloned.1.call-done = bf16[1408,1024]{1,0:T(8,128)(2,1)} async-done(((bf16[1408,128]{1,0:T(8,128)(2,1)}), bf16[1408,1024]{1,0:T(8,128)(2,1)}) %all-gather.17.cloned.1.call-update) | async-done | bytes 2883600 | tf_op jit(solution)/shard_map/all_gather | solution.py:116
  339.3 13.1 %fusion.8 = bf16[1024,1024]{1,0:T(8,128)(2,1)} fusion(bf16[1408,1024]{1,0:T(8,128)(2,1)} %all-gather.17.cloned.1.call-done, f32[1024,1408]{1,0:T(8,128)} %fusion.27, bf16[1024,1024]{1,0:T(8,128)(2,1)} %all-gather.11.cloned.1.call-done, bf16[1024,1408]{1,0:T(8,128)(2,1)} %all-gather.15.cloned.1.call-done), kind=kOutput, calls=%fused_computation.18 | convolution fusion | flops 5915279360 | bytes 15728640 | tf_op jit(solution)/shard_map/dot_general | solution.py:62
  352.4 8.1 %reduce-scatter.2.cloned.1.call-done = bf16[512,1024]{1,0:T(8,128)(2,1)} async-done(((bf16[1024,1024]{1,0:T(8,128)(2,1)}), bf16[512,1024]{1,0:T(8,128)(2,1)}) %reduce-scatter.2.cloned.1.call-update) | async-done | bytes 1048592 | tf_op jit(solution)/shard_map/reduce_scatter | solution.py:120
  360.5 2.5 add_convert_fusion
  (111 shorter events, 21.8 us)
Async XLA Ops:
  6.5 6.4 %copy-start = (bf16[1024,16]{0,1:T(8,128)(2,1)S(1)}, bf16[1024,16]{0,1:T(8,128)(2,1)}, u32[]{:S(2)}) copy-start(bf16[1024,16]{0,1:T(8,128)(2,1)} %param.21) | copy-start | bytes 98308
  6.5 106.0 %all-gather.7.cloned.1.call-start = ((), (), s32[]{:S(2)}) async-start(), calls=%async_computation.2 | async-start | bytes 3145728 | tf_op jit(solution)/shard_map/all_gather | solution.py:85
  6.5 4.2 %copy-start.6 = (bf16[256,128]{1,0:T(8,128)(2,1)S(1)}, bf16[256,128]{1,0:T(8,128)(2,1)}, u32[]{:S(2)}) copy-start(bf16[256,128]{1,0:T(8,128)(2,1)} %param.25) | copy-start | bytes 196612
  8.1 8.7 %copy-start.12 = (bf16[16,128]{1,0:T(8,128)(2,1)S(1)}, bf16[16,128]{1,0:T(8,128)(2,1)}, u32[]{:S(2)}) copy-start(bf16[16,128]{1,0:T(8,128)(2,1)} %param.22) | copy-start | bytes 12292
  8.1 8.7 %copy-start.13 = (f32[128]{0:T(128)S(1)}, f32[128]{0:T(128)}, u32[]{:S(2)}) copy-start(f32[128]{0:T(128)} %param.23) | copy-start | bytes 1540
  10.7 132.1 %all-gather.9.cloned.1.call-start = ((), (), s32[]{:S(2)}) async-start(), calls=%async_computation.3 | async-start | bytes 1179648 | tf_op jit(solution)/shard_map/all_gather | solution.py:108
  13.0 4.6 %copy-start.8 = (bf16[128,128]{1,0:T(8,128)(2,1)S(1)}, bf16[128,128]{1,0:T(8,128)(2,1)}, u32[]{:S(2)}) copy-start(bf16[128,128]{1,0:T(8,128)(2,1)} %param.19) | copy-start | bytes 98308
  14.6 35.6 %copy-start.9 = (bf16[128,128]{1,0:T(8,128)(2,1)S(1)}, bf16[128,128]{1,0:T(8,128)(2,1)}, u32[]{:S(2)}) copy-start(bf16[128,128]{1,0:T(8,128)(2,1)} %param.18) | copy-start | bytes 98308
  14.6 66.6 %copy-start.7 = (bf16[128,256]{1,0:T(8,128)(2,1)S(1)}, bf16[128,256]{1,0:T(8,128)(2,1)}, u32[]{:S(2)}) copy-start(bf16[128,256]{1,0:T(8,128)(2,1)} %param.20) | copy-start | bytes 196612
  112.6 2.5 copy-start.2
  118.1 1.1 copy-start.4
  134.0 3.0 copy-start.5
  137.1 1.2 copy-start.11
  137.8 7.4 %copy-start.1 = (bf16[512,1024]{1,0:T(8,128)(2,1)S(1)}, bf16[512,1024]{1,0:T(8,128)(2,1)}, u32[]{:S(2)}) copy-start(bf16[512,1024]{1,0:T(8,128)(2,1)} %param.16) | copy-start | bytes 3145732
  139.2 5.2 %all-to-all-start = ((bf16[2,512,256]{1,2,0:T(8,128)(2,1)}), bf16[2,512,256]{1,2,0:T(8,128)(2,1)S(1)}, u32[]{:S(2)}, u32[]{:S(2)}) async-start(bf16[2,512,256]{1,2,0:T(8,128)(2,1)} %multiply_convert_fusion.2), calls=%async_computation | async-start | bytes 1048576 | tf_op jit(solution)/shard_map/all_to_all | solution.py:106
  142.7 18.0 %all-gather.11.cloned.1.call-start = ((), (), s32[]{:S(2)}) async-start(), calls=%async_computation.4 | async-start | bytes 3145728 | tf_op jit(solution)/shard_map/all_gather | solution.py:111
  144.4 0.8 copy-start.3
  145.2 2.2 copy-start.10
  148.7 72.5 %all-gather.13.cloned.1.call-start = ((), (), s32[]{:S(2)}) async-start(), calls=%async_computation.5 | async-start | bytes 3244032 | tf_op jit(solution)/shard_map/all_gather | solution.py:113
  149.3 129.9 %all-gather.15.cloned.1.call-start = ((), (), s32[]{:S(2)}) async-start(), calls=%async_computation.6 | async-start | bytes 3244032 | tf_op jit(solution)/shard_map/all_gather | solution.py:114
  149.9 189.5 %all-gather.17.cloned.1.call-start = ((), (), s32[]{:S(2)}) async-start(), calls=%async_computation.7 | async-start | bytes 3244032 | tf_op jit(solution)/shard_map/all_gather | solution.py:116
  150.4 210.1 %reduce-scatter.2.cloned.1.call-start = ((), (), s32[]{:S(2)}) async-start(), calls=%async_computation.8 | async-start | bytes 3145728 | tf_op jit(solution)/shard_map/reduce_scatter | solution.py:120
Sparse Core Ops, SparseCore 0:
  10.8 13.2 all-gather.6
  26.1 42.2 all-gather.8
  148.8 11.8 all-gather.10
  162.7 58.4 all-gather.12
  223.3 55.9 all-gather.14
  281.1 58.1 all-gather.16
  352.5 7.9 reduce-scatter.1
where the time goes:
time: 370 us
  waiting for transfers between devices  192 us (52%)
  blocking collectives  99.3 us (27%)
  matrix products  36.6 us (10%)
  other arithmetic  22.9 us (6%)
  between operations  13.8 us (4%)
  starting transfers between devices  3.91 us (1%)
    all_gather x1, waiting for transfers between devices, local(): lax.all_gather(gate_weight, 'fs', axis=0, tiled=True)  60.5 us
    all_gather x1, waiting for transfers between devices, local(): down_full = lax.all_gather(down_weight, 'fs', axis=1, tiled=True)  60.1 us
    all_gather x1, waiting for transfers between devices, local(): lax.all_gather(up_weight, 'fs', axis=0, tiled=True)  49.6 us
    all_gather x1, blocking collectives, local(): lax.all_gather(key_weight, 'fs', axis=0, tiled=True)  32.6 us
    all_gather x1, blocking collectives, local(): lax.all_gather(value_weight, 'fs', axis=0, tiled=True)  31.3 us
    all_gather x1, blocking collectives, local(): lax.all_gather(query_weight, 'fs', axis=0, tiled=True)  31.1 us
    dot_general x8, matrix products, project_inputs(): return jnp.dot(source, weight, preferred_element_type=jnp.float32)  29.6 us
    dynamic_update_slice x16, other arithmetic, linear_attention(): earlier = lax.scan(advance, initial, (lasting, update))[1]  10.6 us
  transfers between devices with their start and end apart: 8, of which 6 were waited for; matrix products, arithmetic and copies ran while one was open for 10% of the time, Pallas kernels for 0%

commit v1 on v0

--- a/solution.py
+++ b/solution.py
@@ -113,7 +113,12 @@
         lax.all_gather(gate_weight, "fs", axis=0, tiled=True),
         lax.all_gather(up_weight, "fs", axis=0, tiled=True),
     )
-    down_full = lax.all_gather(down_weight, "fs", axis=1, tiled=True)
+    ring = [down_weight]
+    for hop in range(7):
+        ring.append(lax.ppermute(ring[-1], "fs", [(dev, (dev + 1) % 8) for dev in range(8)]))
+    down_full = jnp.roll(
+        jnp.concatenate(ring[::-1], axis=1), (lax.axis_index("fs") + 1) * ring[0].shape[1], axis=1
+    )
     hidden = (
         jax.nn.silu(project_inputs(ffn_sequence, gate_full)) * project_inputs(ffn_sequence, up_full)
     ).astype(jnp.bfloat16)

time: 370 us -> 335 us (0.905)
  waiting for transfers between devices: 192 us -> 133 us
  local copies, waits for them, and re-layouts: 1.33 us -> 22.7 us
    ppermute x0 -> x7, waiting for transfers between devices: none -> 104 us  [local(): lax.ppermute(ring[-1], 'fs', [(dev, (dev + 1) % 8) for dev in range(8)])]
    all_gather x1, waiting for transfers between devices: 60.5 us -> 0.01 us  [local(): lax.all_gather(gate_weight, 'fs', axis=0, tiled=True)]
    all_gather x1 -> x0, waiting for transfers between devices: 60.1 us -> none  [local(): down_full = lax.all_gather(down_weight, 'fs', axis=1, tiled=True)]
    all_gather x1, waiting for transfers between devices: 49.6 us -> 18.4 us  [local(): lax.all_gather(up_weight, 'fs', axis=0, tiled=True)]
    unnamed x28 -> x53, local copies, waits for them, and re-layouts: 0.86 us -> 21.5 us
    all_gather x1, waiting for transfers between devices: 10 us -> 0.01 us  [local(): ffn_sequence = lax.all_gather(ffn_normed, 'tp', axis=0, tiled=True)]
  transfers between devices with their start and end apart: 8 -> 14, of which waited for: 6 -> 10; matrix products, arithmetic and copies ran while one was open for 10% -> 17% of each run, Pallas kernels for 0% -> 0%
where the time goes in v1:
time: 335 us; the launch traced here: 334 us
  waiting for transfers between devices  133 us (40%)
  blocking collectives  99.6 us (30%)
  matrix products  36.6 us (11%)
  other arithmetic  22.9 us (7%)
  local copies, waits for them, and re-layouts  22.7 us (7%)
  between operations  13.8 us (4%)
  starting transfers between devices  5.41 us (2%)
    ppermute x7, waiting for transfers between devices, local(): lax.ppermute(ring[-1], 'fs', [(dev, (dev + 1) % 8) for dev in range(8)])  104 us
    all_gather x1, blocking collectives, local(): lax.all_gather(value_weight, 'fs', axis=0, tiled=True)  33.3 us
    all_gather x1, blocking collectives, local(): lax.all_gather(query_weight, 'fs', axis=0, tiled=True)  31.4 us
    all_gather x1, blocking collectives, local(): lax.all_gather(key_weight, 'fs', axis=0, tiled=True)  30.7 us
    dot_general x8, matrix products, project_inputs(): return jnp.dot(source, weight, preferred_element_type=jnp.float32)  29.5 us
    unnamed x53, local copies, waits for them, and re-layouts  21.5 us
    all_gather x1, waiting for transfers between devices, local(): lax.all_gather(up_weight, 'fs', axis=0, tiled=True)  18.4 us
    dynamic_update_slice x16, other arithmetic, linear_attention(): earlier = lax.scan(advance, initial, (lasting, update))[1]  10.6 us
  transfers between devices with their start and end apart: 14, of which 10 were waited for; matrix products, arithmetic and copies ran while one was open for 17% of the time, Pallas kernels for 0%

profile of v1, /device:TPU:0, one launch (start us, length us, event | category | flops | bytes accessed | tf_op | source)
XLA Modules:
  0.0 334.3 jit_solution(17661143344697548970)
XLA Ops:
  8.1 2.5 fusion.6
  10.7 2.2 all_gather.35
  14.6 2.0 all_gather.33
  17.4 33.3 %all_gather.31 = bf16[1024,256]{1,0:T(8,128)(2,1)S(1)} all-gather(bf16[128,256]{1,0:T(8,128)(2,1)S(1)} %copy-done.12), channel_id=1, replica_groups=mesh['rep'=2,'fs'=8,'tp'=2] {'fs'}, dimensions={0}, use_global_device_ids=true | all-gather | bytes 589824 | tf_op jit(solution)/shard_map/all_gather | solution.py:92
  50.7 31.4 %all_gather.32 = bf16[1024,128]{1,0:T(8,128)(2,1)S(1)} all-gather(bf16[128,128]{1,0:T(8,128)(2,1)S(1)} %copy-done.13), channel_id=1, replica_groups=mesh['rep'=2,'fs'=8,'tp'=2] {'fs'}, dimensions={0}, use_global_device_ids=true | all-gather | bytes 294912 | tf_op jit(solution)/shard_map/all_gather | solution.py:90
  82.1 30.7 %all_gather.34 = bf16[1024,128]{1,0:T(8,128)(2,1)S(1)} all-gather(bf16[128,128]{1,0:T(8,128)(2,1)S(1)} %copy-done.14), channel_id=1, replica_groups=mesh['rep'=2,'fs'=8,'tp'=2] {'fs'}, dimensions={0}, use_global_device_ids=true | all-gather | bytes 294912 | tf_op jit(solution)/shard_map/all_gather | solution.py:91
  112.8 2.4 convolution_convert_fusion.2
  119.5 12.7 %while.13 = (s32[]{:T(128)}, f32[1,128,256]{2,1,0:T(8,128)S(1)}, f32[16,1,128,256]{3,2,1,0:T(8,128)}, f32[16,1,128]{2,1,0:T(1,128)S(1)}, f32[16,1,128,256]{3,2,1,0:T(8,128)S(1)}, /*index=5*/s32[]{:T(128)}, s32[]{:T(128)}) while((s32[]{:T(128)}, f32[1,128,256]{2,1,0:T(8,128)S(1)}, f32[16,1,128,256]{3,2,1,0:T(8,128)}, ...), condition=%wide.region_3.4_spmd.clone, body=%wide.region_2.3_spmd.clone.sunk | while | flops 131075 | bytes 657004 | solution.py:54
  132.1 2.3 convolution_select_fusion
  134.4 3.0 fusion.7
  139.5 3.6 %all-to-all-start = ((bf16[2,512,256]{1,2,0:T(8,128)(2,1)}), bf16[2,512,256]{1,2,0:T(8,128)(2,1)S(1)}, u32[]{:S(2)}, u32[]{:S(2)}) async-start(bf16[2,512,256]{1,2,0:T(8,128)(2,1)} %multiply_convert_fusion.2), calls=%async_computation | async-start | bytes 1048576 | tf_op jit(solution)/shard_map/all_to_all | solution.py:106
  145.7 2.2 multiply_reduce_fusion
  151.4 11.6 %collective-permute-done = bf16[1408,128]{1,0:T(8,128)(2,1)S(1)} collective-permute-done((bf16[1408,128]{1,0:T(8,128)(2,1)S(1)}, bf16[1408,128]{1,0:T(8,128)(2,1)S(1)}, u32[]{:S(2)}, u32[]{:S(2)}) %collective-permute-start) | collective-permute-done | bytes 360480 | tf_op jit(solution)/shard_map/ppermute | solution.py:118
  163.0 12.3 %collective-permute-done.1 = bf16[1408,128]{1,0:T(8,128)(2,1)S(1)} collective-permute-done((bf16[1408,128]{1,0:T(8,128)(2,1)S(1)}, bf16[1408,128]{1,0:T(8,128)(2,1)S(1)}, u32[]{:S(2)}, u32[]{:S(2)}) %collective-permute-start.1) | collective-permute-done | bytes 360480 | tf_op jit(solution)/shard_map/ppermute | solution.py:118
  175.4 20.8 %collective-permute-done.2 = bf16[1408,128]{1,0:T(8,128)(2,1)S(1)} collective-permute-done((bf16[1408,128]{1,0:T(8,128)(2,1)S(1)}, bf16[1408,128]{1,0:T(8,128)(2,1)S(1)}, u32[]{:S(2)}, u32[]{:S(2)}) %collective-permute-start.2) | collective-permute-done | bytes 360480 | tf_op jit(solution)/shard_map/ppermute | solution.py:118
  196.9 16.4 %collective-permute-done.3 = bf16[1408,128]{1,0:T(8,128)(2,1)S(1)} collective-permute-done((bf16[1408,128]{1,0:T(8,128)(2,1)S(1)}, bf16[1408,128]{1,0:T(8,128)(2,1)S(1)}, u32[]{:S(2)}, u32[]{:S(2)}) %collective-permute-start.3) | collective-permute-done | bytes 360480 | tf_op jit(solution)/shard_map/ppermute | solution.py:118
  214.1 19.5 %collective-permute-done.4 = bf16[1408,128]{1,0:T(8,128)(2,1)} collective-permute-done((bf16[1408,128]{1,0:T(8,128)(2,1)S(1)}, bf16[1408,128]{1,0:T(8,128)(2,1)}, u32[]{:S(2)}, u32[]{:S(2)}) %collective-permute-start.4) | collective-permute-done | bytes 360480 | tf_op jit(solution)/shard_map/ppermute | solution.py:118
  233.7 12.5 %collective-permute-done.5 = bf16[1408,128]{1,0:T(8,128)(2,1)} collective-permute-done((bf16[1408,128]{1,0:T(8,128)(2,1)}, bf16[1408,128]{1,0:T(8,128)(2,1)}, u32[]{:S(2)}, u32[]{:S(2)}) %collective-permute-start.5) | collective-permute-done | bytes 360480 | tf_op jit(solution)/shard_map/ppermute | solution.py:118
  246.2 10.4 %collective-permute-done.6 = bf16[1408,128]{1,0:T(8,128)(2,1)} collective-permute-done((bf16[1408,128]{1,0:T(8,128)(2,1)}, bf16[1408,128]{1,0:T(8,128)(2,1)}, u32[]{:S(2)}, u32[]{:S(2)}) %collective-permute-start.6) | collective-permute-done | bytes 360480 | tf_op jit(solution)/shard_map/ppermute | solution.py:118
  276.6 8.3 %fusion.31 = f32[1024,1408]{1,0:T(8,128)} fusion(bf16[1024,1024]{1,0:T(8,128)(2,1)} %all-gather.10.cloned.1.call-done, bf16[1024,1408]{1,0:T(8,128)(2,1)} %all-gather.12.cloned.1.call-done), kind=kOutput, calls=%fused_computation.76 | convolution fusion | flops 2952790016 | bytes 10747904 | tf_op jit(solution)/shard_map/dot_general | solution.py:62
  284.9 18.4 %all-gather.14.cloned.1.call-done = bf16[1024,1408]{1,0:T(8,128)(2,1)} async-done(((bf16[128,1408]{1,0:T(8,128)(2,1)}), bf16[1024,1408]{1,0:T(8,128)(2,1)}) %all-gather.14.cloned.1.call-update) | async-done | bytes 2883600 | tf_op jit(solution)/shard_map/all_gather | solution.py:114
  303.4 13.0 %fusion.9 = bf16[1024,1024]{1,0:T(8,128)(2,1)} fusion(bf16[1408,2048]{1,0:T(8,128)(2,1)} %constant_dynamic-update-slice_fusion, s32[]{:T(128)S(6)} %select_n.28, f32[1024,1408]{1,0:T(8,128)} %fusion.31, bf16[1024,1024]{1,0:T(8,128)(2,1)} %all-gather.10.cloned.1.call-done, bf16[1024,1408]{1,0:T(8,128)(2,1)} %all-gather.14.cloned.1.call-done), kind=kOutput, calls=%fused_computation.19 | convolution fusion | flops 5915279360 | bytes 15728644 | tf_op jit(solution)/shard_map/dot_general | solution.py:62
  316.4 8.5 %reduce-scatter.2.cloned.1.call-done = bf16[512,1024]{1,0:T(8,128)(2,1)} async-done(((bf16[1024,1024]{1,0:T(8,128)(2,1)}), bf16[512,1024]{1,0:T(8,128)(2,1)}) %reduce-scatter.2.cloned.1.call-update) | async-done | bytes 1048592 | tf_op jit(solution)/shard_map/reduce_scatter | solution.py:125
  324.9 2.5 add_convert_fusion
  (148 shorter events, 50.0 us)
Async XLA Ops:
  6.5 6.4 %copy-start = (bf16[1024,16]{0,1:T(8,128)(2,1)S(1)}, bf16[1024,16]{0,1:T(8,128)(2,1)}, u32[]{:S(2)}) copy-start(bf16[1024,16]{0,1:T(8,128)(2,1)} %param.21) | copy-start | bytes 98308
  6.5 106.3 %all-gather.6.cloned.1.call-start = ((), (), s32[]{:S(2)}) async-start(), calls=%async_computation.2 | async-start | bytes 3145728 | tf_op jit(solution)/shard_map/all_gather | solution.py:85
  6.5 10.1 %copy-start.17 = (bf16[16,128]{1,0:T(8,128)(2,1)S(1)}, bf16[16,128]{1,0:T(8,128)(2,1)}, u32[]{:S(2)}) copy-start(bf16[16,128]{1,0:T(8,128)(2,1)} %param.22) | copy-start | bytes 12292
  6.5 10.1 %copy-start.18 = (f32[128]{0:T(128)S(1)}, f32[128]{0:T(128)}, u32[]{:S(2)}) copy-start(f32[128]{0:T(128)} %param.23) | copy-start | bytes 1540
  10.6 6.8 %copy-start.12 = (bf16[128,256]{1,0:T(8,128)(2,1)S(1)}, bf16[128,256]{1,0:T(8,128)(2,1)}, u32[]{:S(2)}) copy-start(bf16[128,256]{1,0:T(8,128)(2,1)} %param.20) | copy-start | bytes 196612
  10.6 40.1 %copy-start.13 = (bf16[128,128]{1,0:T(8,128)(2,1)S(1)}, bf16[128,128]{1,0:T(8,128)(2,1)}, u32[]{:S(2)}) copy-start(bf16[128,128]{1,0:T(8,128)(2,1)} %param.18) | copy-start | bytes 98308
  10.7 71.4 %copy-start.14 = (bf16[128,128]{1,0:T(8,128)(2,1)S(1)}, bf16[128,128]{1,0:T(8,128)(2,1)}, u32[]{:S(2)}) copy-start(bf16[128,128]{1,0:T(8,128)(2,1)} %param.19) | copy-start | bytes 98308
  10.7 132.6 %all-gather.8.cloned.1.call-start = ((), (), s32[]{:S(2)}) async-start(), calls=%async_computation.3 | async-start | bytes 1179648 | tf_op jit(solution)/shard_map/all_gather | solution.py:108
  138.2 7.5 %copy-start.1 = (bf16[512,1024]{1,0:T(8,128)(2,1)S(1)}, bf16[512,1024]{1,0:T(8,128)(2,1)}, u32[]{:S(2)}) copy-start(bf16[512,1024]{1,0:T(8,128)(2,1)} %param.16) | copy-start | bytes 3145732
  139.5 8.4 %copy-start.15 = (f32[1024]{0:T(1024)S(1)}, f32[1024]{0:T(1024)}, u32[]{:S(2)}) copy-start(f32[1024]{0:T(1024)} %param.26) | copy-start | bytes 12292
  139.5 5.4 %all-to-all-start = ((bf16[2,512,256]{1,2,0:T(8,128)(2,1)}), bf16[2,512,256]{1,2,0:T(8,128)(2,1)S(1)}, u32[]{:S(2)}, u32[]{:S(2)}) async-start(bf16[2,512,256]{1,2,0:T(8,128)(2,1)} %multiply_convert_fusion.2), calls=%async_computation | async-start | bytes 1048576 | tf_op jit(solution)/shard_map/all_to_all | solution.py:106
  143.2 133.4 %all-gather.10.cloned.1.call-start = ((), (), s32[]{:S(2)}) async-start(), calls=%async_computation.4 | async-start | bytes 3145728 | tf_op jit(solution)/shard_map/all_gather | solution.py:111
  149.2 127.4 %all-gather.12.cloned.1.call-start = ((), (), s32[]{:S(2)}) async-start(), calls=%async_computation.5 | async-start | bytes 3244032 | tf_op jit(solution)/shard_map/all_gather | solution.py:113
  149.7 153.6 %all-gather.14.cloned.1.call-start = ((), (), s32[]{:S(2)}) async-start(), calls=%async_computation.6 | async-start | bytes 3244032 | tf_op jit(solution)/shard_map/all_gather | solution.py:114
  149.8 13.2 %collective-permute-start = (bf16[1408,128]{1,0:T(8,128)(2,1)S(1)}, bf16[1408,128]{1,0:T(8,128)(2,1)S(1)}, u32[]{:S(2)}, u32[]{:S(2)}) collective-permute-start(bf16[1408,128]{1,0:T(8,128)(2,1)S(1)} %copy-done.6), channel_id=1, source_target_pairs={{0,2},{2,4},{4,6},{6,8},{8,10},{10,12},{12,14},{14,0},{1,3},{3,5},... | collective-permute-start | bytes 1081352 | tf_op jit(solution)/shard_map/ppermute | solution.py:118
  163.0 12.3 %collective-permute-start.1 = (bf16[1408,128]{1,0:T(8,128)(2,1)S(1)}, bf16[1408,128]{1,0:T(8,128)(2,1)S(1)}, u32[]{:S(2)}, u32[]{:S(2)}) collective-permute-start(bf16[1408,128]{1,0:T(8,128)(2,1)S(1)} %collective-permute-done), channel_id=1, source_target_pairs={{0,2},{2,4},{4,6},{6,8},{8,10},{10,12},{12,14},{14,0},{1,3},{3,5},... | collective-permute-start | bytes 1081352 | tf_op jit(solution)/shard_map/ppermute | solution.py:118
  175.3 20.8 %collective-permute-start.2 = (bf16[1408,128]{1,0:T(8,128)(2,1)S(1)}, bf16[1408,128]{1,0:T(8,128)(2,1)S(1)}, u32[]{:S(2)}, u32[]{:S(2)}) collective-permute-start(bf16[1408,128]{1,0:T(8,128)(2,1)S(1)} %collective-permute-done.1), channel_id=1, source_target_pairs={{0,2},{2,4},{4,6},{6,8},{8,10},{10,12},{12,14},{14,0},{1,3},{3,5},... | collective-permute-start | bytes 1081352 | tf_op jit(solution)/shard_map/ppermute | solution.py:118
  196.9 16.4 %collective-permute-start.3 = (bf16[1408,128]{1,0:T(8,128)(2,1)S(1)}, bf16[1408,128]{1,0:T(8,128)(2,1)S(1)}, u32[]{:S(2)}, u32[]{:S(2)}) collective-permute-start(bf16[1408,128]{1,0:T(8,128)(2,1)S(1)} %collective-permute-done.2), channel_id=1, source_target_pairs={{0,2},{2,4},{4,6},{6,8},{8,10},{10,12},{12,14},{14,0},{1,3},{3,5},... | collective-permute-start | bytes 1081352 | tf_op jit(solution)/shard_map/ppermute | solution.py:118
  214.1 19.5 %collective-permute-start.4 = (bf16[1408,128]{1,0:T(8,128)(2,1)S(1)}, bf16[1408,128]{1,0:T(8,128)(2,1)}, u32[]{:S(2)}, u32[]{:S(2)}) collective-permute-start(bf16[1408,128]{1,0:T(8,128)(2,1)S(1)} %collective-permute-done.3), channel_id=1, source_target_pairs={{0,2},{2,4},{4,6},{6,8},{8,10},{10,12},{12,14},{14,0},{1,3},{3,5},... | collective-permute-start | bytes 1081352 | tf_op jit(solution)/shard_map/ppermute | solution.py:118
  233.6 12.6 %collective-permute-start.5 = (bf16[1408,128]{1,0:T(8,128)(2,1)}, bf16[1408,128]{1,0:T(8,128)(2,1)}, u32[]{:S(2)}, u32[]{:S(2)}) collective-permute-start(bf16[1408,128]{1,0:T(8,128)(2,1)} %collective-permute-done.4), channel_id=1, source_target_pairs={{0,2},{2,4},{4,6},{6,8},{8,10},{10,12},{12,14},{14,0},{1,3},{3,5},... | collective-permute-start | bytes 1081352 | tf_op jit(solution)/shard_map/ppermute | solution.py:118
  233.6 91.3 %reduce-scatter.2.cloned.1.call-start = ((), (), s32[]{:S(2)}) async-start(), calls=%async_computation.7 | async-start | bytes 3145728 | tf_op jit(solution)/shard_map/reduce_scatter | solution.py:125
  246.2 10.4 %collective-permute-start.6 = (bf16[1408,128]{1,0:T(8,128)(2,1)}, bf16[1408,128]{1,0:T(8,128)(2,1)}, u32[]{:S(2)}, u32[]{:S(2)}) collective-permute-start(bf16[1408,128]{1,0:T(8,128)(2,1)} %collective-permute-done.5), channel_id=1, source_target_pairs={{0,2},{2,4},{4,6},{6,8},{8,10},{10,12},{12,14},{14,0},{1,3},{3,5},... | collective-permute-start | bytes 1081352 | tf_op jit(solution)/shard_map/ppermute | solution.py:118
  246.2 17.7 %copy-start.8 = (bf16[1408,128]{1,0:T(8,128)(2,1)S(1)}, bf16[1408,128]{1,0:T(8,128)(2,1)}, u32[]{:S(2)}) copy-start(bf16[1408,128]{1,0:T(8,128)(2,1)} %copy-done.7) | copy-start | bytes 1081348
  262.0 10.5 %copy-start.10 = (bf16[1408,128]{1,0:T(8,128)(2,1)S(1)}, bf16[1408,128]{1,0:T(8,128)(2,1)}, u32[]{:S(2)}) copy-start(bf16[1408,128]{1,0:T(8,128)(2,1)} %copy-done.9) | copy-start | bytes 1081348
  (9 other events, 18.4 us)
Sparse Core Ops, SparseCore 0:
  10.8 13.2 all-gather.5
  26.1 42.6 all-gather.7
  149.3 11.5 all-gather.9
  162.9 75.5 all-gather.11
  240.5 62.8 all-gather.13
  316.5 8.3 reduce-scatter.1
